TPU v7x, 32 devices: a whole 2x2x4 slice. The times are simulated.
32 devices in a mesh: sp: 16 (over z, y, core), tp: 2 (over x).
Axes of the slice: x: 2, y: 2, z: 4, core: 2. Of those that a mesh axis runs over, the one named last changes fastest.
Arguments:
- tokens: bfloat16 [1024, 4, 2048], P(('sp', 'tp')), may hold values from -16 to 16
- norm_gain: float32 [2048], replicated, may hold values from 0.1 to 1.9
- w_query: bfloat16 [2048, 2048], P('sp', 'tp'), may hold values from -0.125 to 0.125
- w_forget: bfloat16 [2048, 2048], P('sp', 'tp'), may hold values from -0.125 to 0.125
- w_value: bfloat16 [2048, 2048], P('sp', 'tp'), may hold values from -0.125 to 0.125
- floor_gap: float32 [2048], P('tp'), may hold values from 0 to 0.15, as said below
- head_gain: float32 [2048], P('tp'), may hold values from 0.1 to 1.9
- w_out: bfloat16 [2048, 2048], P('tp', 'sp'), may hold values from -0.125 to 0.125
Outputs:
- mixed: bfloat16 [1024, 4, 2048], P(('sp', 'tp'))
Inputs may be any that keep to these rules, and one draw needn't show every extreme that they name: `floor_gap`: positive, at least 0.5 / 1024 and at most 0.15.
All inputs are finite; a program needn't handle non-finite values.
Results may differ from a plain program's by a relative error of at most 0.014.
Values may be sent and summed in bfloat16 or wider, within the bound.
A program may use at most 128 MiB of HBM per device.

v0:
```python
import math
import jax
import jax.numpy as jnp
from jax import lax
from jax.sharding import PartitionSpec as P

KEY_DIM = 128
VAL_DIM = 128
eps_norm = 1e-06
highest = lax.Precision.HIGHEST


def carried_in(value, axis, combine, identity):
    length, mine = (lax.axis_size(axis), lax.axis_index(axis))
    everything = jax.tree.map(lambda part: lax.all_gather(part, axis), value)
    start = jax.tree.map(
        lambda part, zero: jnp.broadcast_to(jnp.asarray(zero, part.dtype), part.shape),
        value,
        identity,
    )

    def hop(k, before):
        reached = k < mine
        new = combine(before, jax.tree.map(lambda part: part[k], everything))
        return jax.tree.map(lambda a, b: jnp.where(reached, a, b), new, before)

    return lax.fori_loop(0, length, hop, start)


def link_states(earlier, later):
    decay_early, state_early = earlier
    decay_late, state_late = later
    return (decay_early * decay_late, decay_late[..., None] * state_early + state_late)


def local_pass(query, inkey, log_forget, values):
    block_len = query.shape[1]
    cumulative = jnp.cumsum(log_forget, axis=1)
    final = cumulative[:, -1]
    query_scaled = query * jnp.exp(cumulative)
    key_scaled = inkey * jnp.exp(-cumulative)
    key_final = inkey * jnp.exp(final[:, None] - cumulative)
    scores = jnp.einsum("ntshk,nushk->nshtu", query_scaled, key_scaled, precision=highest)
    positions = lax.iota(jnp.int32, block_len)
    causal = positions[:, None] >= positions[None, :]
    scores = jnp.where(causal, scores, 0.0)
    inside = jnp.einsum("nshtu,nushv->ntshv", scores, values, precision=highest)
    updates = jnp.einsum("nushk,nushv->nshkv", key_final, values, precision=highest)
    block_decay = jnp.exp(final)

    def advance(carry, inputs):
        decay_block, update_block = inputs
        return (decay_block[..., None] * carry + update_block, carry)

    end_state, entering = lax.scan(advance, jnp.zeros_like(updates[0]), (block_decay, updates))
    inside = inside + jnp.einsum("ntshk,nshkv->ntshv", query_scaled, entering, precision=highest)
    offsets = jnp.cumsum(final, axis=0) - final
    reach = query_scaled * jnp.exp(offsets)[:, None]
    total_decay = jnp.exp(jnp.sum(final, axis=0))
    return (inside, reach, total_decay, end_state)


def read_out(reach, incoming):
    return jnp.einsum("ntshk,shkv->ntshv", reach, incoming, precision=highest)


def body(tokens, norm_gain, w_query, w_forget, w_value, floor_gap, head_gain, w_out):
    flat = tokens.astype(jnp.float32)
    scale = lax.rsqrt(jnp.mean(flat * flat, axis=-1, keepdims=True) + eps_norm)
    normed = (flat * scale * norm_gain).astype(jnp.bfloat16)
    whole_query, whole_forget, whole_value = (
        lax.all_gather(w_query, "sp", axis=0, tiled=True),
        lax.all_gather(w_forget, "sp", axis=0, tiled=True),
        lax.all_gather(w_value, "sp", axis=0, tiled=True),
    )
    key_width = whole_query.shape[1]
    piece = lax.all_gather(normed, "tp", axis=0, tiled=True)
    flat_rows = piece.reshape(-1, piece.shape[-1])
    outputs = [
        jnp.dot(flat_rows, weight, preferred_element_type=jnp.float32).astype(jnp.bfloat16)
        for weight in (whole_query, whole_forget, whole_value)
    ]
    joined = jnp.concatenate(outputs, axis=1)
    projected = joined.reshape(piece.shape[0], piece.shape[1], joined.shape[1])
    projected = lax.optimization_barrier(projected).astype(jnp.float32)
    positions_dev, sequences = (projected.shape[0], projected.shape[1])
    head_count = key_width // KEY_DIM
    block_len = math.gcd(positions_dev, 128)
    block_count = positions_dev // block_len

    def blocks(value, channels):
        return value.reshape(block_count, block_len, sequences, head_count, channels)

    query = jax.nn.silu(blocks(projected[..., :key_width], KEY_DIM))
    inkey = floor_gap.reshape(head_count, KEY_DIM) * jax.nn.sigmoid(
        -blocks(projected[..., key_width : 2 * key_width], KEY_DIM)
    )
    log_forget = jnp.log1p(-inkey)
    values = blocks(projected[..., 2 * key_width :], VAL_DIM)
    inside, reach, total_decay, end_state = local_pass(query, inkey, log_forget, values)
    _, incoming = carried_in(
        (total_decay, end_state),
        "sp",
        link_states,
        (jnp.ones_like(total_decay), jnp.zeros_like(end_state)),
    )
    recurrent = inside + read_out(reach, incoming)
    mean_square = jnp.mean(recurrent * recurrent, axis=-1, keepdims=True)
    hidden = recurrent * lax.rsqrt(mean_square + eps_norm) * head_gain.reshape(head_count, VAL_DIM)
    hidden = hidden.astype(jnp.bfloat16).reshape(positions_dev, sequences, head_count * VAL_DIM)
    out_columns = lax.all_gather(w_out, "sp", axis=1, tiled=True)
    piece = hidden
    return lax.psum_scatter(
        jnp.einsum("psh,hd->psd", piece, out_columns, preferred_element_type=jnp.float32).astype(
            jnp.bfloat16
        ),
        "tp",
        scatter_dimension=0,
        tiled=True,
    )


def solution(mesh):
    return jax.shard_map(
        body,
        mesh=mesh,
        in_specs=(
            P(("sp", "tp"), None, None),
            P(),
            P("sp", "tp"),
            P("sp", "tp"),
            P("sp", "tp"),
            P("tp"),
            P("tp"),
            P("tp", "sp"),
        ),
        out_specs=P(("sp", "tp"), None, None),
        check_vma=False,
    )
```

profile of v0, /device:TPU:0, one launch (start us, length us, event | category | flops | bytes accessed | tf_op | source)
XLA Modules:
  0.0 463.9 jit_solution(16212869938098595885)
XLA Ops:
  6.5 1.4 fusion.8
  7.9 2.2 fusion.10
  10.2 0.7 all-gather.15.cloned.1.call-update
  10.9 0.7 all-gather.13.cloned.1.call-update
  11.7 0.5 all-gather.11.cloned.1.call-update
  12.3 22.0 %all-gather.9.cloned.1.call-done = bf16[64,4,2048]{2,1,0:T(4,128)(2,1)} async-done(((bf16[32,4,2048]{2,1,0:T(4,128)(2,1)}), bf16[64,4,2048]{2,1,0:T(4,128)(2,1)}) %all-gather.9.cloned.1.call-update) | async-done | bytes 1048592 | tf_op jit(solution)/shard_map/all_gather | solution.py:77
  34.3 1.3 reshape.179
  35.6 51.2 %all-gather.15.cloned.1.call-done = bf16[2048,1024]{1,0:T(8,128)(2,1)} async-done(((bf16[128,1024]{1,0:T(8,128)(2,1)}), bf16[2048,1024]{1,0:T(8,128)(2,1)}) %all-gather.15.cloned.1.call-update) | async-done | bytes 4194320 | tf_op jit(solution)/shard_map/all_gather | solution.py:74
  86.9 3.4 convolution_convert_fusion
  90.3 47.7 %all-gather.13.cloned.1.call-done = bf16[2048,1024]{1,0:T(8,128)(2,1)} async-done(((bf16[128,1024]{1,0:T(8,128)(2,1)}), bf16[2048,1024]{1,0:T(8,128)(2,1)}) %all-gather.13.cloned.1.call-update) | async-done | bytes 4194320 | tf_op jit(solution)/shard_map/all_gather | solution.py:73
  138.0 4.2 convolution_convert_fusion.1
  142.2 46.7 %all-gather.11.cloned.1.call-done = bf16[2048,1024]{1,0:T(8,128)(2,1)} async-done(((bf16[128,1024]{1,0:T(8,128)(2,1)}), bf16[2048,1024]{1,0:T(8,128)(2,1)}) %all-gather.11.cloned.1.call-update) | async-done | bytes 4194320 | tf_op jit(solution)/shard_map/all_gather | solution.py:72
  188.9 3.5 convolution_convert_fusion.2
  192.6 0.6 reshape.180
  193.6 0.6 fusion.12
  194.2 1.4 div.47
  195.6 1.4 div.48
  197.1 1.1 copy-done.4
  198.7 1.5 reshape.182
  200.4 3.8 fusion.17
  204.2 3.7 convolution_add_fusion
  208.8 4.1 convolution_select_fusion
  212.9 0.7 fusion.30
  213.7 2.5 fusion.6
  216.2 21.5 %all-gather = f32[16,1,4,8,128]{4,3,2,1,0:T(8,128)S(1)} all-gather(f32[1,1,4,8,128]{4,3,2,1,0:T(8,128)S(1)} %get-tuple-element.151), channel_id=2, replica_groups=mesh['sp'=16,'tp'=2] {'sp'}, dimensions={0}, use_global_device_ids=true | all-gather | bytes 278528 | tf_op jit(solution)/shard_map/all_gather | solution.py:15
  237.7 139.0 %all-gather.19.cloned.1.call-done = f32[64,8,128,128]{3,2,1,0:T(8,128)} async-done(((f32[4,8,128,128]{3,2,1,0:T(8,128)}), f32[64,8,128,128]{3,2,1,0:T(8,128)}) %all-gather.19.cloned.1.call-update) | async-done | bytes 33554448 | tf_op jit(solution)/shard_map/all_gather | solution.py:15
  376.7 35.5 %while.9 = (s32[]{:T(128)}, f32[4,8,128,128]{3,2,1,0:T(8,128)S(1)}, s32[]{:T(128)}, f32[16,4,8,128]{3,2,1,0:T(8,128)S(1)}, f32[16,4,8,128,128]{4,3,2,1,0:T(8,128)}, /*index=5*/s32[]{:T(128)}, s32[]{:T(128)}) while((s32[]{:T(128)}, f32[4,8,128,128]{3,2,1,0:T(8,128)S(1)}, s32[]{:T(128)}, f32[16,4,8,128]{3,2,1,0:T(8,128)S(1)}, ...), condition=%wide.region_3.4_spmd.clone, body=%wide.region_2.3_spmd.clone.sunk | while | flops 2097156 | bytes 6340721 | solution.py:27
  376.7 2.2 fusion.44
  379.0 2.2 fusion.44
  381.2 2.2 fusion.44
  383.5 2.2 fusion.44
  385.7 2.2 fusion.44
  387.9 2.2 fusion.44
  390.1 2.2 fusion.44
  392.3 2.2 fusion.44
  394.6 2.2 fusion.44
  396.8 2.2 fusion.44
  399.0 2.2 fusion.44
  401.2 2.2 fusion.44
  403.4 2.2 fusion.44
  405.6 2.2 fusion.44
  407.8 2.2 fusion.44
  410.1 2.2 fusion.44
  412.3 3.8 multiply_reduce_fusion
  417.0 14.6 %all-gather.17.cloned.1.call-done = bf16[1024,2048]{1,0:T(8,128)(2,1)} async-done(((bf16[1024,128]{1,0:T(8,128)(2,1)}), bf16[1024,2048]{1,0:T(8,128)(2,1)}) %all-gather.17.cloned.1.call-update) | async-done | bytes 4194320 | tf_op jit(solution)/shard_map/all_gather | solution.py:111
  431.6 4.4 fusion.3
  436.1 18.7 %reduce-scatter.2.cloned.1.call-done = bf16[32,4,2048]{2,0,1:T(8,128)(2,1)} async-done(((bf16[64,4,2048]{2,0,1:T(8,128)(2,1)}), bf16[32,4,2048]{2,0,1:T(8,128)(2,1)}) %reduce-scatter.2.cloned.1.call-update) | async-done | bytes 524304 | tf_op jit(solution)/shard_map/reduce_scatter | solution.py:113
  454.8 2.2 copy.30
  (58 shorter events, 3.4 us)
Async XLA Ops:
  6.5 27.8 %all-gather.9.cloned.1.call-start = ((), (), s32[]{:S(2)}) async-start(), calls=%async_computation.1 | async-start | bytes 1572864 | tf_op jit(solution)/shard_map/all_gather | solution.py:77
  10.1 76.7 %all-gather.15.cloned.1.call-start = ((), (), s32[]{:S(2)}) async-start(), calls=%async_computation.4 | async-start | bytes 4456448 | tf_op jit(solution)/shard_map/all_gather | solution.py:74
  10.9 127.1 %all-gather.13.cloned.1.call-start = ((), (), s32[]{:S(2)}) async-start(), calls=%async_computation.3 | async-start | bytes 4456448 | tf_op jit(solution)/shard_map/all_gather | solution.py:73
  11.6 177.3 %all-gather.11.cloned.1.call-start = ((), (), s32[]{:S(2)}) async-start(), calls=%async_computation.2 | async-start | bytes 4456448 | tf_op jit(solution)/shard_map/all_gather | solution.py:72
  12.2 364.5 %all-gather.19.cloned.1.call-start = ((), (), s32[]{:S(2)}) async-start(), calls=%async_computation.7 | async-start | bytes 35651584 | tf_op jit(solution)/shard_map/all_gather | solution.py:15
  188.9 3.5 copy-start.5
  193.2 3.9 copy-start
  197.0 1.2 copy-start.4
  197.0 1.2 copy-start.6
  198.2 2.0 slice-start
  200.4 3.8 copy-start.1
  207.9 223.7 %all-gather.17.cloned.1.call-start = ((), (), s32[]{:S(2)}) async-start(), calls=%async_computation.5 | async-start | bytes 4456448 | tf_op jit(solution)/shard_map/all_gather | solution.py:111
  208.5 246.3 %reduce-scatter.2.cloned.1.call-start = ((), (), s32[]{:S(2)}) async-start(), calls=%async_computation.6 | async-start | bytes 1572864 | tf_op jit(solution)/shard_map/reduce_scatter | solution.py:113
  208.8 4.1 copy-start.2
  376.7 35.5 %copy-start.3 = (f32[64,4,8,128]{3,2,1,0:T(8,128)S(1)}, f32[64,4,8,128]{3,2,1,0:T(8,128)}, u32[]{:S(2)}) copy-start(f32[64,4,8,128]{3,2,1,0:T(8,128)} %get-tuple-element.147) | copy-start | bytes 3145732
  412.3 3.8 copy-start.7
Sparse Core Ops, SparseCore 0:
  10.3 23.9 all-gather.8
  36.5 50.3 all-gather.14
  89.0 48.8 all-gather.12
  140.0 48.8 all-gather.10
  208.1 168.6 all-gather.18
  378.7 52.8 all-gather.16
  436.2 18.5 reduce-scatter.1
where the time goes:
time: 465 us; the launch traced here: 464 us
  waiting for transfers between devices  343 us (74%)
  other arithmetic  44.1 us (9%)
  matrix products  30.4 us (7%)
  blocking collectives  21.5 us (5%)
  between operations  13.7 us (3%)
  local copies, waits for them, and re-layouts  10.6 us (2%)
    all_gather x1, waiting for transfers between devices, carried_in(): everything = jax.tree.map(lambda part: lax.all_gather(part, axis), value)  139 us
    all_gather x1, waiting for transfers between devices, body(): lax.all_gather(w_value, 'sp', axis=0, tiled=True)  51.2 us
    all_gather x1, waiting for transfers between devices, body(): lax.all_gather(w_forget, 'sp', axis=0, tiled=True)  47.7 us
    all_gather x1, waiting for transfers between devices, body(): lax.all_gather(w_query, 'sp', axis=0, tiled=True)  46.7 us
    select_n x16, other arithmetic, hop(): return jax.tree.map(lambda a, b: jnp.where(reached, a, b), new, before)  34.8 us
    all_gather x1, waiting for transfers between devices, body(): piece = lax.all_gather(normed, 'tp', axis=0, tiled=True)  22 us
    all_gather x1, blocking collectives, carried_in(): everything = jax.tree.map(lambda part: lax.all_gather(part, axis), value)  21.5 us
    reduce_scatter x1, waiting for transfers between devices, body(): lax.psum_scatter(jnp.einsum('psh,hd->psd', piece, out_columns, preferred_...  18.7 us
  transfers between devices with their start and end apart: 7, of which 7 were waited for; matrix products, arithmetic and copies ran while one was open for 12% of the time, Pallas kernels for 0%

commit v1 on v0

--- a/solution.py
+++ b/solution.py
@@ -8,6 +8,19 @@
 VAL_DIM = 128
 eps_norm = 1e-06
 highest = lax.Precision.HIGHEST
+
+
+def gather_around(value, axis, dim):
+    ways = lax.axis_size(axis)
+    up = [(d, (d + 1) % ways) for d in range(ways)]
+    down = [(d, (d - 1) % ways) for d in range(ways)]
+    earlier, later = ([value], [value])
+    for _ in range(ways // 2):
+        earlier.append(lax.ppermute(earlier[-1], axis, up))
+    for _ in range((ways - 1) // 2):
+        later.append(lax.ppermute(later[-1], axis, down))
+    line = jnp.concatenate([*earlier[::-1], *later[1:]], axis=dim)
+    return jnp.roll(line, (lax.axis_index(axis) - ways // 2) * value.shape[dim], axis=dim)
 
 
 def carried_in(value, axis, combine, identity):
@@ -71,7 +84,7 @@
     whole_query, whole_forget, whole_value = (
         lax.all_gather(w_query, "sp", axis=0, tiled=True),
         lax.all_gather(w_forget, "sp", axis=0, tiled=True),
-        lax.all_gather(w_value, "sp", axis=0, tiled=True),
+        gather_around(w_value, "sp", 0),
     )
     key_width = whole_query.shape[1]
     piece = lax.all_gather(normed, "tp", axis=0, tiled=True)

time: 465 us -> 428 us (0.920)
  waiting for transfers between devices: 343 us -> 262 us
  starting transfers between devices: 0.42 us -> 33.3 us
  local copies, waits for them, and re-layouts: 10.6 us -> 19.8 us
    all_gather x1 -> x0, waiting for transfers between devices: 51.2 us -> none  [body(): lax.all_gather(w_value, 'sp', axis=0, tiled=True)]
    all_gather x1, waiting for transfers between devices: 47.7 us -> 0.02 us  [body(): lax.all_gather(w_forget, 'sp', axis=0, tiled=True)]
    ppermute x0 -> x15, waiting for transfers between devices: none -> 43.4 us  [the longest x8 30.5 us: gather_around(): earlier.append(lax.ppermute(earlier[-1], axis, up))]
    ppermute x0 -> x15, starting transfers between devices: none -> 32.9 us  [the longest x7 32.4 us: gather_around(): later.append(lax.ppermute(later[-1], axis, down))]
    all_gather x1, waiting for transfers between devices: 22 us -> 0.01 us  [body(): piece = lax.all_gather(normed, 'tp', axis=0, tiled=True)]
    unnamed x16 -> x49, local copies, waits for them, and re-layouts: 1.11 us -> 10.2 us
  transfers between devices with their start and end apart: 7 -> 21, of which waited for: 7 -> 16; matrix products, arithmetic and copies ran while one was open for 12% -> 15% of each run, Pallas kernels for 0% -> 0%
where the time goes in v1:
time: 428 us; the launch traced here: 427 us
  waiting for transfers between devices  262 us (61%)
  other arithmetic  46.3 us (11%)
  starting transfers between devices  33.3 us (8%)
  matrix products  29.4 us (7%)
  blocking collectives  21.4 us (5%)
  local copies, waits for them, and re-layouts  19.8 us (5%)
  between operations  14 us (3%)
    all_gather x1, waiting for transfers between devices, carried_in(): everything = jax.tree.map(lambda part: lax.all_gather(part, axis), value)  138 us
    all_gather x1, waiting for transfers between devices, body(): lax.all_gather(w_query, 'sp', axis=0, tiled=True)  45.4 us
    select_n x16, other arithmetic, hop(): return jax.tree.map(lambda a, b: jnp.where(reached, a, b), new, before)  34.8 us
    ppermute x7, starting transfers between devices, gather_around(): later.append(lax.ppermute(later[-1], axis, down))  32.4 us
    ppermute x8, waiting for transfers between devices, gather_around(): earlier.append(lax.ppermute(earlier[-1], axis, up))  30.5 us
    all_gather x1, blocking collectives, carried_in(): everything = jax.tree.map(lambda part: lax.all_gather(part, axis), value)  21.4 us
    reduce_scatter x1, waiting for transfers between devices, body(): lax.psum_scatter(jnp.einsum('psh,hd->psd', piece, out_columns, preferred_...  18.7 us
    all_gather x1, waiting for transfers between devices, body(): out_columns = lax.all_gather(w_out, 'sp', axis=1, tiled=True)  14.6 us
  transfers between devices with their start and end apart: 21, of which 16 were waited for; matrix products, arithmetic and copies ran while one was open for 15% of the time, Pallas kernels for 0%

profile of v1, /device:TPU:0, one launch (start us, length us, event | category | flops | bytes accessed | tf_op | source)
XLA Modules:
  0.0 426.9 jit_solution(6281294413000104947)
XLA Ops:
  8.0 2.2 fusion.15
  12.3 9.2 %collective-permute-done = bf16[128,1024]{1,0:T(8,128)(2,1)S(1)} collective-permute-done((bf16[128,1024]{1,0:T(8,128)(2,1)}, bf16[128,1024]{1,0:T(8,128)(2,1)S(1)}, u32[]{:S(2)}, u32[]{:S(2)}) %collective-permute-start) | collective-permute-done | bytes 262176 | tf_op jit(solution)/shard_map/ppermute | solution.py:19
  21.5 4.4 %collective-permute-start.8 = (bf16[128,1024]{1,0:T(8,128)(2,1)}, bf16[128,1024]{1,0:T(8,128)(2,1)S(1)}, u32[]{:S(2)}, u32[]{:S(2)}) collective-permute-start(bf16[128,1024]{1,0:T(8,128)(2,1)} %param.14), channel_id=1, source_target_pairs={{0,30},{2,0},{4,2},{6,4},{8,6},{10,8},{12,10},{14,12},{16,14},{18,... | collective-permute-start | bytes 786440 | tf_op jit(solution)/shard_map/ppermute | solution.py:21
  26.0 4.1 collective-permute-done.1
  30.2 4.6 %collective-permute-start.9 = (bf16[128,1024]{1,0:T(8,128)(2,1)S(1)}, bf16[128,1024]{1,0:T(8,128)(2,1)S(1)}, u32[]{:S(2)}, u32[]{:S(2)}) collective-permute-start(bf16[128,1024]{1,0:T(8,128)(2,1)S(1)} %collective-permute-done.8), channel_id=1, source_target_pairs={{0,30},{2,0},{4,2},{6,4},{8,6},{10,8},{12,10},{14,12},{16,14},{18,... | collective-permute-start | bytes 786440 | tf_op jit(solution)/shard_map/ppermute | solution.py:21
  34.8 3.8 collective-permute-done.2
  38.7 4.7 %collective-permute-start.10 = (bf16[128,1024]{1,0:T(8,128)(2,1)S(1)}, bf16[128,1024]{1,0:T(8,128)(2,1)S(1)}, u32[]{:S(2)}, u32[]{:S(2)}) collective-permute-start(bf16[128,1024]{1,0:T(8,128)(2,1)S(1)} %collective-permute-done.9), channel_id=1, source_target_pairs={{0,30},{2,0},{4,2},{6,4},{8,6},{10,8},{12,10},{14,12},{16,14},{18,... | collective-permute-start | bytes 786440 | tf_op jit(solution)/shard_map/ppermute | solution.py:21
  43.4 3.8 collective-permute-done.3
  47.2 3.9 collective-permute-done.10
  51.1 4.6 %collective-permute-start.11 = (bf16[128,1024]{1,0:T(8,128)(2,1)S(1)}, bf16[128,1024]{1,0:T(8,128)(2,1)S(1)}, u32[]{:S(2)}, u32[]{:S(2)}) collective-permute-start(bf16[128,1024]{1,0:T(8,128)(2,1)S(1)} %collective-permute-done.10), channel_id=1, source_target_pairs={{0,30},{2,0},{4,2},{6,4},{8,6},{10,8},{12,10},{14,12},{16,14},{18,... | collective-permute-start | bytes 786440 | tf_op jit(solution)/shard_map/ppermute | solution.py:21
  57.6 2.4 collective-permute-done.11
  60.0 4.6 %collective-permute-start.12 = (bf16[128,1024]{1,0:T(8,128)(2,1)S(1)}, bf16[128,1024]{1,0:T(8,128)(2,1)}, u32[]{:S(2)}, u32[]{:S(2)}) collective-permute-start(bf16[128,1024]{1,0:T(8,128)(2,1)S(1)} %collective-permute-done.11), channel_id=1, source_target_pairs={{0,30},{2,0},{4,2},{6,4},{8,6},{10,8},{12,10},{14,12},{16,14},{18,... | collective-permute-start | bytes 786440 | tf_op jit(solution)/shard_map/ppermute | solution.py:21
  66.2 6.4 %collective-permute-done.12 = bf16[128,1024]{1,0:T(8,128)(2,1)} collective-permute-done((bf16[128,1024]{1,0:T(8,128)(2,1)S(1)}, bf16[128,1024]{1,0:T(8,128)(2,1)}, u32[]{:S(2)}, u32[]{:S(2)}) %collective-permute-start.12) | collective-permute-done | bytes 262176 | tf_op jit(solution)/shard_map/ppermute | solution.py:21
  72.5 4.7 %collective-permute-start.13 = (bf16[128,1024]{1,0:T(8,128)(2,1)}, bf16[128,1024]{1,0:T(8,128)(2,1)}, u32[]{:S(2)}, u32[]{:S(2)}) collective-permute-start(bf16[128,1024]{1,0:T(8,128)(2,1)} %collective-permute-done.12), channel_id=1, source_target_pairs={{0,30},{2,0},{4,2},{6,4},{8,6},{10,8},{12,10},{14,12},{16,14},{18,... | collective-permute-start | bytes 786440 | tf_op jit(solution)/shard_map/ppermute | solution.py:21
  77.2 3.0 collective-permute-done.6
  81.6 4.7 %collective-permute-start.14 = (bf16[128,1024]{1,0:T(8,128)(2,1)}, bf16[128,1024]{1,0:T(8,128)(2,1)S(1)}, u32[]{:S(2)}, u32[]{:S(2)}) collective-permute-start(bf16[128,1024]{1,0:T(8,128)(2,1)} %collective-permute-done.13), channel_id=1, source_target_pairs={{0,30},{2,0},{4,2},{6,4},{8,6},{10,8},{12,10},{14,12},{16,14},{18,... | collective-permute-start | bytes 786440 | tf_op jit(solution)/shard_map/ppermute | solution.py:21
  86.3 3.1 collective-permute-done.7
  101.1 4.2 convolution_convert_fusion
  105.4 45.4 %all-gather.10.cloned.1.call-done = bf16[2048,1024]{1,0:T(8,128)(2,1)} async-done(((bf16[128,1024]{1,0:T(8,128)(2,1)}), bf16[2048,1024]{1,0:T(8,128)(2,1)}) %all-gather.10.cloned.1.call-update) | async-done | bytes 4194320 | tf_op jit(solution)/shard_map/all_gather | solution.py:85
  150.7 3.4 convolution_convert_fusion.1
  163.4 3.8 fusion.22
  167.2 3.7 convolution_add_fusion
  171.9 4.1 convolution_select_fusion
  177.9 2.5 fusion.8
  180.3 21.4 %all-gather = f32[16,1,4,8,128]{4,3,2,1,0:T(8,128)S(1)} all-gather(f32[1,1,4,8,128]{4,3,2,1,0:T(8,128)S(1)} %get-tuple-element.151), channel_id=2, replica_groups=mesh['sp'=16,'tp'=2] {'sp'}, dimensions={0}, use_global_device_ids=true | all-gather | bytes 278528 | tf_op jit(solution)/shard_map/all_gather | solution.py:28
  201.7 138.0 %all-gather.16.cloned.1.call-done = f32[64,8,128,128]{3,2,1,0:T(8,128)} async-done(((f32[4,8,128,128]{3,2,1,0:T(8,128)}), f32[64,8,128,128]{3,2,1,0:T(8,128)}) %all-gather.16.cloned.1.call-update) | async-done | bytes 33554448 | tf_op jit(solution)/shard_map/all_gather | solution.py:28
  339.8 35.5 %while.9 = (s32[]{:T(128)}, f32[4,8,128,128]{3,2,1,0:T(8,128)S(1)}, s32[]{:T(128)}, f32[16,4,8,128]{3,2,1,0:T(8,128)S(1)}, f32[16,4,8,128,128]{4,3,2,1,0:T(8,128)}, /*index=5*/s32[]{:T(128)}, s32[]{:T(128)}) while((s32[]{:T(128)}, f32[4,8,128,128]{3,2,1,0:T(8,128)S(1)}, s32[]{:T(128)}, f32[16,4,8,128]{3,2,1,0:T(8,128)S(1)}, ...), condition=%wide.region_3.4_spmd.clone, body=%wide.region_2.3_spmd.clone.sunk | while | flops 2097156 | bytes 6340721 | solution.py:40
  339.8 2.2 fusion.49
  342.1 2.2 fusion.49
  344.3 2.2 fusion.49
  346.5 2.2 fusion.49
  348.7 2.2 fusion.49
  351.0 2.2 fusion.49
  353.2 2.2 fusion.49
  355.4 2.2 fusion.49
  357.6 2.2 fusion.49
  359.8 2.2 fusion.49
  362.0 2.2 fusion.49
  364.2 2.2 fusion.49
  366.4 2.2 fusion.49
  368.7 2.2 fusion.49
  370.9 2.2 fusion.49
  373.1 2.2 fusion.49
  375.3 3.8 multiply_reduce_fusion
  380.0 14.6 %all-gather.14.cloned.1.call-done = bf16[1024,2048]{1,0:T(8,128)(2,1)} async-done(((bf16[1024,128]{1,0:T(8,128)(2,1)}), bf16[1024,2048]{1,0:T(8,128)(2,1)}) %all-gather.14.cloned.1.call-update) | async-done | bytes 4194320 | tf_op jit(solution)/shard_map/all_gather | solution.py:124
  394.6 4.4 %fusion.5 = bf16[64,4,2048]{2,0,1:T(8,128)(2,1)} fusion(bf16[64,4,1024]{2,0,1:T(8,128)(2,1)S(1)} %reshape.183, bf16[1024,2048]{1,0:T(8,128)(2,1)} %all-gather.14.cloned.1.call-done), kind=kOutput, calls=%fused_computation.7 | convolution fusion | flops 1074266112 | bytes 5767168 | tf_op jit(solution)/shard_map/psh,hd->psd/dot_general | solution.py:127
  399.1 18.7 %reduce-scatter.2.cloned.1.call-done = bf16[32,4,2048]{2,0,1:T(8,128)(2,1)} async-done(((bf16[64,4,2048]{2,0,1:T(8,128)(2,1)}), bf16[32,4,2048]{2,0,1:T(8,128)(2,1)}) %reduce-scatter.2.cloned.1.call-update) | async-done | bytes 524304 | tf_op jit(solution)/shard_map/reduce_scatter | solution.py:126
  417.8 2.2 copy.30
  (118 shorter events, 33.0 us)
Async XLA Ops:
  6.5 86.9 %copy-start.2 = (bf16[128,1024]{1,0:T(8,128)(2,1)S(1)}, bf16[128,1024]{1,0:T(8,128)(2,1)}, u32[]{:S(2)}) copy-start(bf16[128,1024]{1,0:T(8,128)(2,1)} %param.14) | copy-start | bytes 786436
  6.5 73.7 %all-gather.8.cloned.1.call-start = ((), (), s32[]{:S(2)}) async-start(), calls=%async_computation.1 | async-start | bytes 1572864 | tf_op jit(solution)/shard_map/all_gather | solution.py:90
  10.2 90.9 %all-gather.12.cloned.1.call-start = ((), (), s32[]{:S(2)}) async-start(), calls=%async_computation.3 | async-start | bytes 4456448 | tf_op jit(solution)/shard_map/all_gather | solution.py:86
  10.9 139.8 %all-gather.10.cloned.1.call-start = ((), (), s32[]{:S(2)}) async-start(), calls=%async_computation.2 | async-start | bytes 4456448 | tf_op jit(solution)/shard_map/all_gather | solution.py:85
  11.7 328.1 %all-gather.16.cloned.1.call-start = ((), (), s32[]{:S(2)}) async-start(), calls=%async_computation.6 | async-start | bytes 35651584 | tf_op jit(solution)/shard_map/all_gather | solution.py:28
  11.7 9.8 %collective-permute-start = (bf16[128,1024]{1,0:T(8,128)(2,1)}, bf16[128,1024]{1,0:T(8,128)(2,1)S(1)}, u32[]{:S(2)}, u32[]{:S(2)}) collective-permute-start(bf16[128,1024]{1,0:T(8,128)(2,1)} %param.14), channel_id=1, source_target_pairs={{0,2},{2,4},{4,6},{6,8},{8,10},{10,12},{12,14},{14,16},{16,18},{18... | collective-permute-start | bytes 786440 | tf_op jit(solution)/shard_map/ppermute | solution.py:19
  21.5 8.5 %collective-permute-start.1 = (bf16[128,1024]{1,0:T(8,128)(2,1)S(1)}, bf16[128,1024]{1,0:T(8,128)(2,1)S(1)}, u32[]{:S(2)}, u32[]{:S(2)}) collective-permute-start(bf16[128,1024]{1,0:T(8,128)(2,1)S(1)} %collective-permute-done), channel_id=1, source_target_pairs={{0,2},{2,4},{4,6},{6,8},{8,10},{10,12},{12,14},{14,16},{16,18},{18... | collective-permute-start | bytes 786440 | tf_op jit(solution)/shard_map/ppermute | solution.py:19
  21.5 8.6 %collective-permute-start.8 = (bf16[128,1024]{1,0:T(8,128)(2,1)}, bf16[128,1024]{1,0:T(8,128)(2,1)S(1)}, u32[]{:S(2)}, u32[]{:S(2)}) collective-permute-start(bf16[128,1024]{1,0:T(8,128)(2,1)} %param.14), channel_id=1, source_target_pairs={{0,30},{2,0},{4,2},{6,4},{8,6},{10,8},{12,10},{14,12},{16,14},{18,... | collective-permute-start | bytes 786440 | tf_op jit(solution)/shard_map/ppermute | solution.py:21
  30.0 8.6 %collective-permute-start.2 = (bf16[128,1024]{1,0:T(8,128)(2,1)S(1)}, bf16[128,1024]{1,0:T(8,128)(2,1)S(1)}, u32[]{:S(2)}, u32[]{:S(2)}) collective-permute-start(bf16[128,1024]{1,0:T(8,128)(2,1)S(1)} %collective-permute-done.1), channel_id=1, source_target_pairs={{0,2},{2,4},{4,6},{6,8},{8,10},{10,12},{12,14},{14,16},{16,18},{18... | collective-permute-start | bytes 786440 | tf_op jit(solution)/shard_map/ppermute | solution.py:19
  30.2 8.5 %collective-permute-start.9 = (bf16[128,1024]{1,0:T(8,128)(2,1)S(1)}, bf16[128,1024]{1,0:T(8,128)(2,1)S(1)}, u32[]{:S(2)}, u32[]{:S(2)}) collective-permute-start(bf16[128,1024]{1,0:T(8,128)(2,1)S(1)} %collective-permute-done.8), channel_id=1, source_target_pairs={{0,30},{2,0},{4,2},{6,4},{8,6},{10,8},{12,10},{14,12},{16,14},{18,... | collective-permute-start | bytes 786440 | tf_op jit(solution)/shard_map/ppermute | solution.py:21
  38.6 8.6 %collective-permute-start.3 = (bf16[128,1024]{1,0:T(8,128)(2,1)S(1)}, bf16[128,1024]{1,0:T(8,128)(2,1)S(1)}, u32[]{:S(2)}, u32[]{:S(2)}) collective-permute-start(bf16[128,1024]{1,0:T(8,128)(2,1)S(1)} %collective-permute-done.2), channel_id=1, source_target_pairs={{0,2},{2,4},{4,6},{6,8},{8,10},{10,12},{12,14},{14,16},{16,18},{18... | collective-permute-start | bytes 786440 | tf_op jit(solution)/shard_map/ppermute | solution.py:19
  38.7 12.4 %collective-permute-start.10 = (bf16[128,1024]{1,0:T(8,128)(2,1)S(1)}, bf16[128,1024]{1,0:T(8,128)(2,1)S(1)}, u32[]{:S(2)}, u32[]{:S(2)}) collective-permute-start(bf16[128,1024]{1,0:T(8,128)(2,1)S(1)} %collective-permute-done.9), channel_id=1, source_target_pairs={{0,30},{2,0},{4,2},{6,4},{8,6},{10,8},{12,10},{14,12},{16,14},{18,... | collective-permute-start | bytes 786440 | tf_op jit(solution)/shard_map/ppermute | solution.py:21
  47.2 10.4 %collective-permute-start.4 = (bf16[128,1024]{1,0:T(8,128)(2,1)S(1)}, bf16[128,1024]{1,0:T(8,128)(2,1)S(1)}, u32[]{:S(2)}, u32[]{:S(2)}) collective-permute-start(bf16[128,1024]{1,0:T(8,128)(2,1)S(1)} %collective-permute-done.3), channel_id=1, source_target_pairs={{0,2},{2,4},{4,6},{6,8},{8,10},{10,12},{12,14},{14,16},{16,18},{18... | collective-permute-start | bytes 786440 | tf_op jit(solution)/shard_map/ppermute | solution.py:19
  51.1 8.9 %collective-permute-start.11 = (bf16[128,1024]{1,0:T(8,128)(2,1)S(1)}, bf16[128,1024]{1,0:T(8,128)(2,1)S(1)}, u32[]{:S(2)}, u32[]{:S(2)}) collective-permute-start(bf16[128,1024]{1,0:T(8,128)(2,1)S(1)} %collective-permute-done.10), channel_id=1, source_target_pairs={{0,30},{2,0},{4,2},{6,4},{8,6},{10,8},{12,10},{14,12},{16,14},{18,... | collective-permute-start | bytes 786440 | tf_op jit(solution)/shard_map/ppermute | solution.py:21
  57.6 15.0 %copy-start.3 = (bf16[128,1024]{1,0:T(8,128)(2,1)}, bf16[128,1024]{1,0:T(8,128)(2,1)S(1)}, u32[]{:S(2)}) copy-start(bf16[128,1024]{1,0:T(8,128)(2,1)S(1)} %collective-permute-done.4) | copy-start | bytes 786436
  57.6 8.6 %collective-permute-start.5 = (bf16[128,1024]{1,0:T(8,128)(2,1)S(1)}, bf16[128,1024]{1,0:T(8,128)(2,1)S(1)}, u32[]{:S(2)}, u32[]{:S(2)}) collective-permute-start(bf16[128,1024]{1,0:T(8,128)(2,1)S(1)} %collective-permute-done.4), channel_id=1, source_target_pairs={{0,2},{2,4},{4,6},{6,8},{8,10},{10,12},{12,14},{14,16},{16,18},{18... | collective-permute-start | bytes 786440 | tf_op jit(solution)/shard_map/ppermute | solution.py:19
  60.0 12.5 %collective-permute-start.12 = (bf16[128,1024]{1,0:T(8,128)(2,1)S(1)}, bf16[128,1024]{1,0:T(8,128)(2,1)}, u32[]{:S(2)}, u32[]{:S(2)}) collective-permute-start(bf16[128,1024]{1,0:T(8,128)(2,1)S(1)} %collective-permute-done.11), channel_id=1, source_target_pairs={{0,30},{2,0},{4,2},{6,4},{8,6},{10,8},{12,10},{14,12},{16,14},{18,... | collective-permute-start | bytes 786440 | tf_op jit(solution)/shard_map/ppermute | solution.py:21
  66.1 11.1 %copy-start.5 = (bf16[128,1024]{1,0:T(8,128)(2,1)}, bf16[128,1024]{1,0:T(8,128)(2,1)S(1)}, u32[]{:S(2)}) copy-start(bf16[128,1024]{1,0:T(8,128)(2,1)S(1)} %collective-permute-done.5) | copy-start | bytes 786436
  66.1 14.1 %collective-permute-start.6 = (bf16[128,1024]{1,0:T(8,128)(2,1)S(1)}, bf16[128,1024]{1,0:T(8,128)(2,1)}, u32[]{:S(2)}, u32[]{:S(2)}) collective-permute-start(bf16[128,1024]{1,0:T(8,128)(2,1)S(1)} %collective-permute-done.5), channel_id=1, source_target_pairs={{0,2},{2,4},{4,6},{6,8},{8,10},{10,12},{12,14},{14,16},{16,18},{18... | collective-permute-start | bytes 786440 | tf_op jit(solution)/shard_map/ppermute | solution.py:19
  72.5 9.1 %collective-permute-start.13 = (bf16[128,1024]{1,0:T(8,128)(2,1)}, bf16[128,1024]{1,0:T(8,128)(2,1)}, u32[]{:S(2)}, u32[]{:S(2)}) collective-permute-start(bf16[128,1024]{1,0:T(8,128)(2,1)} %collective-permute-done.12), channel_id=1, source_target_pairs={{0,30},{2,0},{4,2},{6,4},{8,6},{10,8},{12,10},{14,12},{16,14},{18,... | collective-permute-start | bytes 786440 | tf_op jit(solution)/shard_map/ppermute | solution.py:21
  80.2 9.2 %collective-permute-start.7 = (bf16[128,1024]{1,0:T(8,128)(2,1)}, bf16[128,1024]{1,0:T(8,128)(2,1)}, u32[]{:S(2)}, u32[]{:S(2)}) collective-permute-start(bf16[128,1024]{1,0:T(8,128)(2,1)} %collective-permute-done.6), channel_id=1, source_target_pairs={{0,2},{2,4},{4,6},{6,8},{8,10},{10,12},{12,14},{14,16},{16,18},{18... | collective-permute-start | bytes 786440 | tf_op jit(solution)/shard_map/ppermute | solution.py:19
  81.6 15.9 %copy-start.6 = (bf16[128,1024]{1,0:T(8,128)(2,1)S(1)}, bf16[128,1024]{1,0:T(8,128)(2,1)}, u32[]{:S(2)}) copy-start(bf16[128,1024]{1,0:T(8,128)(2,1)} %copy-done.5) | copy-start | bytes 786436
  81.6 15.9 %copy-start.4 = (bf16[128,1024]{1,0:T(8,128)(2,1)S(1)}, bf16[128,1024]{1,0:T(8,128)(2,1)}, u32[]{:S(2)}) copy-start(bf16[128,1024]{1,0:T(8,128)(2,1)} %copy-done.3) | copy-start | bytes 786436
  81.6 13.9 %collective-permute-start.14 = (bf16[128,1024]{1,0:T(8,128)(2,1)}, bf16[128,1024]{1,0:T(8,128)(2,1)S(1)}, u32[]{:S(2)}, u32[]{:S(2)}) collective-permute-start(bf16[128,1024]{1,0:T(8,128)(2,1)} %collective-permute-done.13), channel_id=1, source_target_pairs={{0,30},{2,0},{4,2},{6,4},{8,6},{10,8},{12,10},{14,12},{16,14},{18,... | collective-permute-start | bytes 786440 | tf_op jit(solution)/shard_map/ppermute | solution.py:21
  155.3 4.7 %copy-start.7 = (f32[1024]{0:T(1024)S(1)}, f32[1024]{0:T(1024)}, u32[]{:S(2)}) copy-start(f32[1024]{0:T(1024)} %param.15) | copy-start | bytes 12292
  163.4 8.4 %copy-start = (bf16[64,4,8,128]{3,2,1,0:T(8,128)(2,1)}, bf16[64,4,8,128]{3,2,1,0:T(8,128)(2,1)S(1)}, u32[]{:S(2)}) copy-start(bf16[64,4,8,128]{3,2,1,0:T(8,128)(2,1)S(1)} %reshape.187) | copy-start | bytes 1572868
  171.0 223.7 %all-gather.14.cloned.1.call-start = ((), (), s32[]{:S(2)}) async-start(), calls=%async_computation.4 | async-start | bytes 4456448 | tf_op jit(solution)/shard_map/all_gather | solution.py:124
  171.6 246.3 %reduce-scatter.2.cloned.1.call-start = ((), (), s32[]{:S(2)}) async-start(), calls=%async_computation.5 | async-start | bytes 1572864 | tf_op jit(solution)/shard_map/reduce_scatter | solution.py:126
  339.8 35.5 %copy-start.1 = (f32[64,4,8,128]{3,2,1,0:T(8,128)S(1)}, f32[64,4,8,128]{3,2,1,0:T(8,128)}, u32[]{:S(2)}) copy-start(f32[64,4,8,128]{3,2,1,0:T(8,128)} %get-tuple-element.147) | copy-start | bytes 3145732
  339.8 39.3 %copy-start.8 = (f32[1024]{0:T(1024)S(1)}, f32[1024]{0:T(1024)}, u32[]{:S(2)}) copy-start(f32[1024]{0:T(1024)} %param.16) | copy-start | bytes 12292
Sparse Core Ops, SparseCore 0:
  10.3 23.9 all-gather.7
  36.5 58.6 all-gather.11
  97.4 53.2 all-gather.9
  171.1 168.6 all-gather.15
  341.8 52.8 all-gather.13
  399.2 18.5 reduce-scatter.1
